TPU v7x, 32 devices: a whole 2x2x4 slice. The times are simulated.
32 devices in a mesh: fs: 8 (over z, x), tp: 4 (over y, core).
Axes of the slice: x: 2, y: 2, z: 4, core: 2. Of those that a mesh axis runs over, the one named last changes fastest.
Arguments:
- tokens: bfloat16 [8192, 2048], P(('fs', 'tp')), may hold values from -130 to 130
- pool_weight: bfloat16 [4, 512, 512], P(None, 'fs'), may hold values from -0.25 to 0.25
- pool_scale: float32 [2048], replicated, may hold values from 0.5 to 1.5
- gain_mix: float32 [2048], replicated, may hold values from 0.1 to 1.9
- gain_mlp: float32 [2048], replicated, may hold values from 0.1 to 1.9
- w_up: bfloat16 [8192, 2048], P('tp', 'fs'), may hold values from -0.125 to 0.125
- w_down: bfloat16 [8192, 2048], P('tp', 'fs'), may hold values from -0.0625 to 0.0625
- gain_out: float32 [2048], P('tp'), may hold values from 0.1 to 1.9
Outputs:
- result: bfloat16 [8192, 2048], P('fs', 'tp')
All inputs are finite; a program needn't handle non-finite values.
Results may differ from a plain program's by a relative error of at most 0.013.
Values may be sent and summed in bfloat16 or wider, within the bound.
A program may use at most 64 MiB of HBM per device.

v0:
```python
import jax
import jax.numpy as jnp
from jax import lax
from jax.sharding import PartitionSpec as P

D = 2048
SEQ_LEN = 1024
EPS = 1e-06
WINDOWS = (2, 4, 8, 16)


def extended_2(x, sides, width):
    for axis, dim in sides:
        peers, length = (lax.axis_size(axis), x.shape[dim])
        up = [(i, (i + 1) % peers) for i in range(peers - 1)]
        down = [(j, i) for i, j in up]
        last = lax.slice_in_dim(x, length - width, length, axis=dim)
        first = lax.slice_in_dim(x, 0, width, axis=dim)
        before = lax.ppermute(last, axis, up)
        after = lax.ppermute(first, axis, down)
        x = jnp.concatenate([before, x, after], axis=dim)
    return x


def rms_scale(values, gain):
    return values * lax.rsqrt(jnp.mean(values * values, axis=-1, keepdims=True) + EPS) * gain


def local(tokens, pool_weight, pool_scale, gain_mix, gain_mlp, w_up, w_down, gain_out):
    rows = tokens.shape[0]
    width = tokens.shape[1]
    group = width // 4
    offset = lax.axis_index("tp") * rows
    inputs = tokens.astype(jnp.float32)
    normed = rms_scale(inputs, gain_mix).astype(jnp.bfloat16)
    extended = extended_2(normed, (("tp", 0),), 8).astype(jnp.float32)
    line = jnp.arange(rows + 16, dtype=jnp.int32)
    lower_open = offset % SEQ_LEN != 0
    upper_open = (offset + rows) % SEQ_LEN != 0
    keep = jnp.where(line < 8, lower_open, jnp.where(line >= rows + 8, upper_open, True))
    level = extended * keep.astype(jnp.float32)[:, None]
    position = (offset + jnp.arange(rows, dtype=jnp.int32)) % SEQ_LEN
    normed_f32 = normed.astype(jnp.float32)
    full_pool = lax.all_gather(pool_weight, "fs", axis=1, tiled=True)
    pieces = []
    for index, reach in enumerate(WINDOWS):
        half = reach // 2
        level = level[:-half] + level[half:]
        start = 8 - half
        window = level[start : start + rows, :group]
        lower = jnp.maximum(position - half, 0)
        upper = jnp.minimum(position + half, SEQ_LEN)
        counts = (upper - lower).astype(jnp.float32)[:, None]
        own = normed_f32[:, index * group : (index + 1) * group]
        pooled = (window / counts - own).astype(jnp.bfloat16)
        pieces.append(jnp.dot(pooled, full_pool[index], preferred_element_type=jnp.float32))
        level = level[:, group:]
    mixed = jnp.concatenate(pieces, axis=1) * pool_scale
    first_sum = (inputs + mixed).astype(jnp.bfloat16)
    inner = rms_scale(first_sum.astype(jnp.float32), gain_mlp).astype(jnp.bfloat16)
    all_inner = lax.all_gather(inner, "tp", axis=0, tiled=True)
    contract = (((1,), (1,)), ((), ()))
    pre = lax.dot_general(
        all_inner,
        lax.all_gather(w_up, "fs", axis=1, tiled=True),
        contract,
        preferred_element_type=jnp.float32,
    )
    hidden = jnp.square(jax.nn.relu(pre)).astype(jnp.bfloat16)
    partial_terms = jnp.dot(
        hidden, lax.all_gather(w_down, "fs", axis=1, tiled=True), preferred_element_type=jnp.float32
    )
    channel_out = lax.psum_scatter(
        partial_terms.astype(jnp.bfloat16), "tp", scatter_dimension=1, tiled=True
    ).astype(jnp.float32)
    first_columns = lax.all_to_all(first_sum, "tp", split_axis=1, concat_axis=0, tiled=True)
    second_sum = first_columns.astype(jnp.float32) + channel_out
    squares = lax.psum(jnp.sum(second_sum * second_sum, axis=1), "tp")
    scaled = second_sum * lax.rsqrt(squares / D + EPS)[:, None] * gain_out
    return scaled.astype(jnp.bfloat16)


def solution(mesh):
    return jax.shard_map(
        local,
        mesh=mesh,
        in_specs=(
            P(("fs", "tp"), None),
            P(None, "fs", None),
            P(),
            P(),
            P(),
            P("tp", "fs"),
            P("tp", "fs"),
            P("tp"),
        ),
        out_specs=P("fs", "tp"),
        check_vma=False,
    )
```

profile of v0, /device:TPU:0, one launch (start us, length us, event | category | flops | bytes accessed | tf_op | source)
XLA Modules:
  0.0 437.5 jit_solution(9384960922146906074)
XLA Ops:
  6.5 0.7 all-gather.5.cloned.1.call-update
  7.3 1.5 fusion.3
  8.8 2.9 fusion.30
  11.7 2.4 collective-permute-start
  14.1 1.3 collective-permute-start.1
  15.5 3.8 collective-permute-done.1
  20.1 1.2 copy-done.1
  21.4 1.1 fusion.32
  22.6 38.8 %all-gather.5.cloned.1.call-done = bf16[4,512,512]{2,1,0:T(8,128)(2,1)} async-done(((bf16[4,64,512]{2,1,0:T(8,128)(2,1)}), bf16[4,512,512]{2,1,0:T(8,128)(2,1)}) %all-gather.5.cloned.1.call-update) | async-done | bytes 2097168 | tf_op jit(solution)/shard_map/all_gather | solution.py:44
  61.3 1.7 fusion.14
  63.2 1.7 fusion.12
  65.4 0.6 copy-done.4
  66.7 0.5 fusion
  67.4 1.3 fusion.2
  68.7 0.7 all-gather.9.cloned.1.call-update
  70.0 31.8 %all-gather.7.cloned.1.call-done = bf16[1024,2048]{1,0:T(8,128)(2,1)} async-done(((bf16[256,2048]{1,0:T(8,128)(2,1)}), bf16[1024,2048]{1,0:T(8,128)(2,1)}) %all-gather.7.cloned.1.call-update) | async-done | bytes 4194320 | tf_op jit(solution)/shard_map/all_gather | solution.py:61
  101.8 127.0 %all-gather.9.cloned.1.call-done = bf16[2048,2048]{1,0:T(8,128)(2,1)} async-done(((bf16[2048,256]{1,0:T(8,128)(2,1)}), bf16[2048,2048]{1,0:T(8,128)(2,1)}) %all-gather.9.cloned.1.call-update) | async-done | bytes 8388624 | tf_op jit(solution)/shard_map/all_gather | solution.py:65
  228.8 125.0 %all-gather.11.cloned.1.call-done = bf16[2048,2048]{1,0:T(8,128)(2,1)} async-done(((bf16[2048,256]{1,0:T(8,128)(2,1)}), bf16[2048,2048]{1,0:T(8,128)(2,1)}) %all-gather.11.cloned.1.call-update) | async-done | bytes 8388624 | tf_op jit(solution)/shard_map/all_gather | solution.py:71
  353.9 25.5 %convolution_convert_fusion = bf16[1024,2048]{1,0:T(8,128)(2,1)} fusion(bf16[2048,2048]{1,0:T(8,128)(2,1)} %all-gather.11.cloned.1.call-done, bf16[1024,2048]{1,0:T(8,128)(2,1)} %all-gather.7.cloned.1.call-done, bf16[2048,2048]{1,0:T(8,128)(2,1)} %all-gather.9.cloned.1.call-done), kind=kOutput, calls=%fused_computation.1 | convolution fusion | flops 17188257792 | bytes 25165824 | tf_op jit(solution)/shard_map/dot_general | solution.py:70
  379.5 17.0 %all_to_all.13 = bf16[256,4,512]{2,0,1:T(8,128)(2,1)S(1)} all-to-all(bf16[256,4,512]{2,0,1:T(8,128)(2,1)S(1)} %bitcast.28), channel_id=1, replica_groups=mesh['fs'=8,'tp'=4] {'tp'}, dimensions={1} | all-to-all | bytes 2097152 | tf_op jit(solution)/shard_map/all_to_all | solution.py:76
  396.5 25.6 %reduce-scatter.2.cloned.1.call-done = bf16[1024,512]{1,0:T(8,128)(2,1)} async-done(((bf16[1024,2048]{1,0:T(8,128)(2,1)}), bf16[1024,512]{1,0:T(8,128)(2,1)}) %reduce-scatter.2.cloned.1.call-update) | async-done | bytes 1048592 | tf_op jit(solution)/shard_map/reduce_scatter | solution.py:73
  422.1 1.7 multiply_reduce_fusion
  423.8 5.8 %psum.7 = f32[1024]{0:T(1024)S(1)} all-reduce(f32[1024]{0:T(1024)S(1)} %multiply_reduce_fusion), channel_id=1, replica_groups=mesh['fs'=8,'tp'=4] {'tp'}, use_global_device_ids=true, to_apply=%region_4.5 | all-reduce | flops 1024 | bytes 8192 | tf_op jit(solution)/shard_map/psum | solution.py:78
  429.6 1.4 multiply_convert_fusion.1
  (41 shorter events, 3.2 us)
Async XLA Ops:
  6.5 54.8 %all-gather.5.cloned.1.call-start = ((), (), s32[]{:S(2)}) async-start(), calls=%async_computation.2 | async-start | bytes 2359296 | tf_op jit(solution)/shard_map/all_gather | solution.py:44
  7.3 94.6 %all-gather.7.cloned.1.call-start = ((), (), s32[]{:S(2)}) async-start(), calls=%async_computation.3 | async-start | bytes 5242880 | tf_op jit(solution)/shard_map/all_gather | solution.py:61
  11.7 3.8 collective-permute-start
  14.1 5.2 %collective-permute-start.1 = (bf16[8,2048]{1,0:T(8,128)(2,1)S(1)}, bf16[8,2048]{1,0:T(8,128)(2,1)S(1)}, u32[]{:S(2)}, u32[]{:S(2)}) collective-permute-start(bf16[8,2048]{1,0:T(8,128)(2,1)S(1)} %get-tuple-element.12), channel_id=1, source_target_pairs={{1,0},{2,1},{3,2},{5,4},{6,5},{7,6},{9,8},{10,9},{11,10},{13,12},{... | collective-permute-start | bytes 98312 | tf_op jit(solution)/shard_map/ppermute | solution.py:20
  20.1 1.2 copy-start.1
  61.3 1.9 copy-start.3
  63.0 2.0 copy-start.9
  64.9 1.1 copy-start.4
  64.9 1.2 copy-start.5
  65.4 1.3 copy-start
  65.4 1.3 copy-start.6
  66.7 0.7 copy-start.7
  68.7 160.2 %all-gather.9.cloned.1.call-start = ((), (), s32[]{:S(2)}) async-start(), calls=%async_computation.4 | async-start | bytes 9437184 | tf_op jit(solution)/shard_map/all_gather | solution.py:65
  69.4 284.5 %all-gather.11.cloned.1.call-start = ((), (), s32[]{:S(2)}) async-start(), calls=%async_computation.5 | async-start | bytes 9437184 | tf_op jit(solution)/shard_map/all_gather | solution.py:71
  70.0 352.1 %reduce-scatter.2.cloned.1.call-start = ((), (), s32[]{:S(2)}) async-start(), calls=%async_computation.6 | async-start | bytes 5242880 | tf_op jit(solution)/shard_map/reduce_scatter | solution.py:73
  379.5 50.1 %copy-start.8 = (f32[512]{0:T(512)S(1)}, f32[512]{0:T(512)}, u32[]{:S(2)}) copy-start(f32[512]{0:T(512)} %param.15) | copy-start | bytes 6148
  422.1 7.5 %copy-start.2 = (bf16[1024,512]{1,0:T(8,128)(2,1)S(1)}, bf16[1024,512]{1,0:T(8,128)(2,1)}, u32[]{:S(2)}) copy-start(bf16[1024,512]{1,0:T(8,128)(2,1)} %reduce-scatter.2.cloned.1.call-done) | copy-start | bytes 3145732
Sparse Core Ops, SparseCore 0:
  9.5 51.7 all-gather.4
  68.8 32.9 all-gather.6
  103.9 124.9 all-gather.8
  230.7 123.1 all-gather.10
  379.5 42.5 reduce-scatter.1
where the time goes:
time: 438 us
  waiting for transfers between devices  354 us (81%)
  matrix products  29.5 us (7%)
  blocking collectives  22.8 us (5%)
  between operations  13.3 us (3%)
  other arithmetic  10.2 us (2%)
    all_gather x1, waiting for transfers between devices, local(): lax.all_gather(w_up, 'fs', axis=1, tiled=True)  127 us
    all_gather x1, waiting for transfers between devices, local(): lax.all_gather(w_down, 'fs', axis=1, tiled=True)  125 us
    all_gather x1, waiting for transfers between devices, local(): full_pool = lax.all_gather(pool_weight, 'fs', axis=1, tiled=True)  38.8 us
    all_gather x1, waiting for transfers between devices, local(): all_inner = lax.all_gather(inner, 'tp', axis=0, tiled=True)  31.8 us
    reduce_scatter x1, waiting for transfers between devices, local(): lax.psum_scatter(partial_terms.astype(jnp.bfloat16), 'tp', scatter_dimens...  25.6 us
    dot_general x1, matrix products, local(): jnp.dot(hidden, lax.all_gather(w_down, 'fs', axis=1, tiled=True), preferr...  25.5 us
    all_to_all x1, blocking collectives, local(): lax.all_to_all(first_sum, 'tp', split_axis=1, concat_axis=0, tiled=True)  17 us
  transfers between devices with their start and end apart: 7, of which 6 were waited for; matrix products, arithmetic and copies ran while one was open for 1% of the time, Pallas kernels for 0%

commit v1 on v0

--- a/solution.py
+++ b/solution.py
@@ -7,6 +7,17 @@
 SEQ_LEN = 1024
 EPS = 1e-06
 WINDOWS = (2, 4, 8, 16)
+
+
+def gather_by_hops(array, mesh_axis, d):
+    size = lax.axis_size(mesh_axis)
+    route = [(i, (i + 1) % size) for i in range(size)]
+    shards = [array]
+    for reach in range(1, size):
+        shards = [lax.ppermute(shards[0], mesh_axis, route), *shards]
+    out = jnp.concatenate(shards, axis=d)
+    offset = (lax.axis_index(mesh_axis) + 1) * shards[-1].shape[d]
+    return jnp.roll(out, offset, axis=d)
 
 
 def extended_2(x, sides, width):
@@ -58,7 +69,7 @@
     mixed = jnp.concatenate(pieces, axis=1) * pool_scale
     first_sum = (inputs + mixed).astype(jnp.bfloat16)
     inner = rms_scale(first_sum.astype(jnp.float32), gain_mlp).astype(jnp.bfloat16)
-    all_inner = lax.all_gather(inner, "tp", axis=0, tiled=True)
+    all_inner = gather_by_hops(inner, "tp", 0)
     contract = (((1,), (1,)), ((), ()))
     pre = lax.dot_general(
         all_inner,

time: 438 us -> 396 us (0.904)
  waiting for transfers between devices: 354 us -> 303 us
  local copies, waits for them, and re-layouts: 3.79 us -> 13.6 us
    all_gather x1, waiting for transfers between devices: 127 us -> 64.7 us  [local(): lax.all_gather(w_up, 'fs', axis=1, tiled=True)]
    ppermute x0 -> x3, waiting for transfers between devices: none -> 42.8 us  [gather_by_hops(): shards = [lax.ppermute(shards[0], mesh_axis, route), *shards]]
    all_gather x1 -> x0, waiting for transfers between devices: 31.8 us -> none  [local(): all_inner = lax.all_gather(inner, 'tp', axis=0, tiled=True)]
    unnamed x20 -> x30, local copies, waits for them, and re-layouts: 2.56 us -> 12.4 us
  transfers between devices with their start and end apart: 7 -> 9, of which waited for: 6 -> 8; matrix products, arithmetic and copies ran while one was open for 1% -> 5% of each run, Pallas kernels for 0% -> 0%
where the time goes in v1:
time: 396 us
  waiting for transfers between devices  303 us (77%)
  matrix products  29.7 us (8%)
  blocking collectives  22.8 us (6%)
  local copies, waits for them, and re-layouts  13.6 us (3%)
  between operations  13.4 us (3%)
  other arithmetic  9.4 us (2%)
    all_gather x1, waiting for transfers between devices, local(): lax.all_gather(w_down, 'fs', axis=1, tiled=True)  125 us
    all_gather x1, waiting for transfers between devices, local(): lax.all_gather(w_up, 'fs', axis=1, tiled=True)  64.7 us
    ppermute x3, waiting for transfers between devices, gather_by_hops(): shards = [lax.ppermute(shards[0], mesh_axis, route), *shards]  42.8 us
    all_gather x1, waiting for transfers between devices, local(): full_pool = lax.all_gather(pool_weight, 'fs', axis=1, tiled=True)  38.7 us
    reduce_scatter x1, waiting for transfers between devices, local(): lax.psum_scatter(partial_terms.astype(jnp.bfloat16), 'tp', scatter_dimens...  25.6 us
    dot_general x1, matrix products, local(): jnp.dot(hidden, lax.all_gather(w_down, 'fs', axis=1, tiled=True), preferr...  25.5 us
    all_to_all x1, blocking collectives, local(): lax.all_to_all(first_sum, 'tp', split_axis=1, concat_axis=0, tiled=True)  17 us
    unnamed x30, local copies, waits for them, and re-layouts  12.4 us
  transfers between devices with their start and end apart: 9, of which 8 were waited for; matrix products, arithmetic and copies ran while one was open for 5% of the time, Pallas kernels for 0%

profile of v1, /device:TPU:0, one launch (start us, length us, event | category | flops | bytes accessed | tf_op | source)
XLA Modules:
  0.0 395.7 jit_solution(4421293765592188307)
XLA Ops:
  9.1 1.6 fusion.39
  10.7 2.4 collective-permute-start
  13.1 1.3 collective-permute-start.1
  14.5 3.8 collective-permute-done.1
  19.1 1.2 copy-done.1
  21.5 1.1 fusion.41
  22.6 38.7 %all-gather.4.cloned.1.call-done = bf16[4,512,512]{2,1,0:T(8,128)(2,1)} async-done(((bf16[4,64,512]{2,1,0:T(8,128)(2,1)}), bf16[4,512,512]{2,1,0:T(8,128)(2,1)}) %all-gather.4.cloned.1.call-update) | async-done | bytes 2097168 | tf_op jit(solution)/shard_map/all_gather | solution.py:55
  61.3 1.9 fusion.19
  63.4 1.7 fusion.17
  67.8 14.2 %collective-permute-done.2 = bf16[256,2048]{1,0:T(8,128)(2,1)S(1)} collective-permute-done((bf16[256,2048]{1,0:T(8,128)(2,1)S(1)}, bf16[256,2048]{1,0:T(8,128)(2,1)S(1)}, u32[]{:S(2)}, u32[]{:S(2)}) %collective-permute-start.2) | collective-permute-done | bytes 1048608 | tf_op jit(solution)/shard_map/ppermute | solution.py:17
  82.0 14.2 %collective-permute-done.3 = bf16[256,2048]{1,0:T(8,128)(2,1)S(1)} collective-permute-done((bf16[256,2048]{1,0:T(8,128)(2,1)S(1)}, bf16[256,2048]{1,0:T(8,128)(2,1)S(1)}, u32[]{:S(2)}, u32[]{:S(2)}) %collective-permute-start.3) | collective-permute-done | bytes 1048608 | tf_op jit(solution)/shard_map/ppermute | solution.py:17
  96.2 14.3 %collective-permute-done.4 = bf16[256,2048]{1,0:T(8,128)(2,1)} collective-permute-done((bf16[256,2048]{1,0:T(8,128)(2,1)S(1)}, bf16[256,2048]{1,0:T(8,128)(2,1)}, u32[]{:S(2)}, u32[]{:S(2)}) %collective-permute-start.4) | collective-permute-done | bytes 1048608 | tf_op jit(solution)/shard_map/ppermute | solution.py:17
  110.5 2.3 constant_dynamic-update-slice_fusion.7
  115.0 1.3 constant_dynamic-update-slice_fusion.4
  116.3 2.4 constant_dynamic-update-slice_fusion.3
  120.8 1.3 constant_dynamic-update-slice_fusion
  122.2 64.7 %all-gather.6.cloned.1.call-done = bf16[2048,2048]{1,0:T(8,128)(2,1)} async-done(((bf16[2048,256]{1,0:T(8,128)(2,1)}), bf16[2048,2048]{1,0:T(8,128)(2,1)}) %all-gather.6.cloned.1.call-update) | async-done | bytes 8388624 | tf_op jit(solution)/shard_map/all_gather | solution.py:76
  186.9 125.2 %all-gather.8.cloned.1.call-done = bf16[2048,2048]{1,0:T(8,128)(2,1)} async-done(((bf16[2048,256]{1,0:T(8,128)(2,1)}), bf16[2048,2048]{1,0:T(8,128)(2,1)}) %all-gather.8.cloned.1.call-update) | async-done | bytes 8388624 | tf_op jit(solution)/shard_map/all_gather | solution.py:82
  312.1 25.5 %fusion.4 = bf16[1024,2048]{1,0:T(8,128)(2,1)} fusion(bf16[2048,2048]{1,0:T(8,128)(2,1)} %all-gather.8.cloned.1.call-done, bf16[2048,2048]{1,0:T(8,128)(2,1)} %all-gather.6.cloned.1.call-done, bf16[2048,2048]{1,0:T(8,128)(2,1)} %constant_dynamic-update-slice_fusion, s32[]{:T(128)S(6)} %select_n.64), kind=kOutput, calls=%fused_computation.3 | convolution fusion | flops 17188257792 | bytes 25165828 | tf_op jit(solution)/shard_map/dot_general | solution.py:81
  337.7 17.0 %all_to_all.13 = bf16[256,4,512]{2,0,1:T(8,128)(2,1)S(1)} all-to-all(bf16[256,4,512]{2,0,1:T(8,128)(2,1)S(1)} %bitcast.27), channel_id=1, replica_groups=mesh['fs'=8,'tp'=4] {'tp'}, dimensions={1} | all-to-all | bytes 2097152 | tf_op jit(solution)/shard_map/all_to_all | solution.py:87
  354.7 25.6 %reduce-scatter.2.cloned.1.call-done = bf16[1024,512]{1,0:T(8,128)(2,1)} async-done(((bf16[1024,2048]{1,0:T(8,128)(2,1)}), bf16[1024,512]{1,0:T(8,128)(2,1)}) %reduce-scatter.2.cloned.1.call-update) | async-done | bytes 1048592 | tf_op jit(solution)/shard_map/reduce_scatter | solution.py:84
  380.3 1.7 multiply_reduce_fusion
  382.0 5.8 %psum.7 = f32[1024]{0:T(1024)S(1)} all-reduce(f32[1024]{0:T(1024)S(1)} %multiply_reduce_fusion), channel_id=1, replica_groups=mesh['fs'=8,'tp'=4] {'tp'}, use_global_device_ids=true, to_apply=%region_4.5 | all-reduce | flops 1024 | bytes 8192 | tf_op jit(solution)/shard_map/psum | solution.py:89
  387.8 1.4 multiply_convert_fusion.1
  (56 shorter events, 11.7 us)
Async XLA Ops:
  6.5 2.3 copy-start
  6.5 2.6 copy-start.8
  6.5 54.8 %all-gather.4.cloned.1.call-start = ((), (), s32[]{:S(2)}) async-start(), calls=%async_computation.2 | async-start | bytes 2359296 | tf_op jit(solution)/shard_map/all_gather | solution.py:55
  7.3 179.6 %all-gather.6.cloned.1.call-start = ((), (), s32[]{:S(2)}) async-start(), calls=%async_computation.3 | async-start | bytes 9437184 | tf_op jit(solution)/shard_map/all_gather | solution.py:76
  8.0 304.1 %all-gather.8.cloned.1.call-start = ((), (), s32[]{:S(2)}) async-start(), calls=%async_computation.4 | async-start | bytes 9437184 | tf_op jit(solution)/shard_map/all_gather | solution.py:82
  8.7 371.6 %reduce-scatter.2.cloned.1.call-start = ((), (), s32[]{:S(2)}) async-start(), calls=%async_computation.5 | async-start | bytes 5242880 | tf_op jit(solution)/shard_map/reduce_scatter | solution.py:84
  10.7 3.8 collective-permute-start
  13.1 5.2 %collective-permute-start.1 = (bf16[8,2048]{1,0:T(8,128)(2,1)S(1)}, bf16[8,2048]{1,0:T(8,128)(2,1)S(1)}, u32[]{:S(2)}, u32[]{:S(2)}) collective-permute-start(bf16[8,2048]{1,0:T(8,128)(2,1)S(1)} %get-tuple-element.12), channel_id=1, source_target_pairs={{1,0},{2,1},{3,2},{5,4},{6,5},{7,6},{9,8},{10,9},{11,10},{13,12},{... | collective-permute-start | bytes 98312 | tf_op jit(solution)/shard_map/ppermute | solution.py:31
  19.1 1.2 copy-start.1
  20.5 1.0 copy-start.2
  61.3 2.1 copy-start.4
  63.2 2.0 copy-start.11
  65.1 1.1 copy-start.5
  65.1 1.2 copy-start.6
  65.5 1.1 copy-start.9
  66.7 0.7 copy-start.7
  67.7 14.3 %collective-permute-start.2 = (bf16[256,2048]{1,0:T(8,128)(2,1)S(1)}, bf16[256,2048]{1,0:T(8,128)(2,1)S(1)}, u32[]{:S(2)}, u32[]{:S(2)}) collective-permute-start(bf16[256,2048]{1,0:T(8,128)(2,1)S(1)} %fusion.9), channel_id=1, source_target_pairs={{0,1},{1,2},{2,3},{3,0},{4,5},{5,6},{6,7},{7,4},{8,9},{9,10},{10,1... | collective-permute-start | bytes 3145736 | tf_op jit(solution)/shard_map/ppermute | solution.py:17
  82.0 14.2 %collective-permute-start.3 = (bf16[256,2048]{1,0:T(8,128)(2,1)S(1)}, bf16[256,2048]{1,0:T(8,128)(2,1)S(1)}, u32[]{:S(2)}, u32[]{:S(2)}) collective-permute-start(bf16[256,2048]{1,0:T(8,128)(2,1)S(1)} %collective-permute-done.2), channel_id=1, source_target_pairs={{0,1},{1,2},{2,3},{3,0},{4,5},{5,6},{6,7},{7,4},{8,9},{9,10},{10,1... | collective-permute-start | bytes 3145736 | tf_op jit(solution)/shard_map/ppermute | solution.py:17
  96.2 14.3 %collective-permute-start.4 = (bf16[256,2048]{1,0:T(8,128)(2,1)S(1)}, bf16[256,2048]{1,0:T(8,128)(2,1)}, u32[]{:S(2)}, u32[]{:S(2)}) collective-permute-start(bf16[256,2048]{1,0:T(8,128)(2,1)S(1)} %collective-permute-done.3), channel_id=1, source_target_pairs={{0,1},{1,2},{2,3},{3,0},{4,5},{5,6},{6,7},{7,4},{8,9},{9,10},{10,1... | collective-permute-start | bytes 3145736 | tf_op jit(solution)/shard_map/ppermute | solution.py:17
  337.7 50.1 %copy-start.10 = (f32[512]{0:T(512)S(1)}, f32[512]{0:T(512)}, u32[]{:S(2)}) copy-start(f32[512]{0:T(512)} %param.15) | copy-start | bytes 6148
  380.3 7.5 %copy-start.3 = (bf16[1024,512]{1,0:T(8,128)(2,1)S(1)}, bf16[1024,512]{1,0:T(8,128)(2,1)}, u32[]{:S(2)}) copy-start(bf16[1024,512]{1,0:T(8,128)(2,1)} %reduce-scatter.2.cloned.1.call-done) | copy-start | bytes 3145732
Sparse Core Ops, SparseCore 0:
  9.5 51.7 all-gather.3
  63.4 123.4 all-gather.5
  188.9 123.1 all-gather.7
  337.7 42.5 reduce-scatter.1
